TPU v7x, 512 devices: a 4x2x32 block of a 4x8x32 slice. The times are simulated.
512 devices in a mesh: grp: 2 (over y), fs: 32 (over z), tp: 8 (over x, core).
Axes of the slice: x: 4, y: 2, z: 32, core: 2. Of those that a mesh axis runs over, the one named last changes fastest.
The devices are a block of a 4x8x32 slice.
Arguments:
- tokens: bfloat16 [64, 384, 2048], P(('grp', 'fs'), None, 'tp'), parts along dimension 0, may hold values from -24 to 24
- input_gain: float32 [2048], replicated, may hold values from 0.1 to 1.9
- query_weight: bfloat16 [2048, 1024], P('fs', 'tp'), may hold values from -0.125 to 0.125
- key_weight: bfloat16 [2048, 1024], P('fs', 'tp'), may hold values from -0.125 to 0.125
- value_weight: bfloat16 [2048, 1024], P('fs', 'tp'), may hold values from -0.125 to 0.125
- output_gate_matrix: bfloat16 [2048, 1024], P('fs', 'tp'), may hold values from -0.125 to 0.125
- forward_decay: float32 [16], P('tp'), may hold values from -1 to 9
- backward_decay: float32 [16], P('tp'), may hold values from -1 to 9
- merge_weight: bfloat16 [1024, 2048], P('tp', 'fs'), may hold values from -0.375 to 0.375
- middle_gain: float32 [2048], replicated, may hold values from 0.1 to 1.9
- gate_weight: bfloat16 [2048, 5120], P('fs', 'tp'), may hold values from -0.125 to 0.125
- up_weight: bfloat16 [2048, 5120], P('fs', 'tp'), may hold values from -0.125 to 0.125
- down_weight: bfloat16 [5120, 2048], P('tp', 'fs'), may hold values from -0.15625 to 0.15625
Outputs:
- layer_out: bfloat16 [64, 384, 2048], P(('grp', 'fs'), None, 'tp'), parts along dimension 0
There are 2 independent parts, one for each index of `grp`. A program takes and returns all parts, laid end to end along the dimension named above; an argument that names none is the same for every part. Nothing has to cross between parts.
All inputs are finite; a program needn't handle non-finite values.
Results may differ from a plain program's by a relative error of at most 0.019.
Values may be sent and summed in bfloat16 or wider, within the bound.
A program may use at most 64 MiB of HBM per device.

v0:
```python
import jax
import jax.numpy as jnp
from jax import lax
from jax.sharding import PartitionSpec as P

BLOCK = 128


norm_eps = 1e-06
group_eps = 1e-05
rope_base = 10000.0
highest_precision = lax.Precision.HIGHEST


def joined_along(tiles, dim):
    tiles = jnp.moveaxis(tiles, 0, dim)
    lengths = tiles.shape
    return tiles.reshape(*lengths[:dim], lengths[dim] * lengths[dim + 1], *lengths[dim + 2 :])


def copy_for_each(array, axis):
    copies = jnp.broadcast_to(array, (lax.axis_size(axis), *array.shape))
    return lax.all_to_all(copies, axis, split_axis=0, concat_axis=0, tiled=True)


def gathered_copies(array, axis, dim):
    return joined_along(copy_for_each(array, axis), dim)


def sent_together(arrays, axis, dim, along):
    both = jnp.concatenate(arrays, axis=along)
    result, at, gathered = (lax.all_gather(both, axis, axis=dim, tiled=True), 0, [])
    for a in arrays:
        gathered.append(lax.slice_in_dim(result, at, at + a.shape[along], axis=along))
        at += a.shape[along]
    return tuple(gathered)


def split_up(array, dim, peers):
    lengths = array.shape
    tiles = array.reshape(*lengths[:dim], peers, lengths[dim] // peers, *lengths[dim + 1 :])
    return jnp.moveaxis(tiles, dim, 0)


def summed_on_arrival(array, axis, dim):
    peers = lax.axis_size(axis)
    tiles = lax.all_to_all(split_up(array, dim, peers), axis, 0, 0, tiled=True)
    return jnp.sum(tiles.astype(jnp.float32), axis=0)


def rms_scale(values, gain_vector):
    widened = values.astype(jnp.float32)
    scaled = widened * lax.rsqrt(jnp.mean(widened * widened, axis=-1, keepdims=True) + norm_eps)
    return (scaled * gain_vector).astype(jnp.bfloat16)


def apply_rotary_heads(values, length):
    half_dim = values.shape[-1] // 2
    inverse = rope_base ** (-jnp.arange(half_dim, dtype=jnp.float32) / half_dim)
    angles = jnp.arange(length, dtype=jnp.float32)[:, None] * inverse[None, :]
    cosine = jnp.cos(angles)[:, None, :]
    sine_part = jnp.sin(angles)[:, None, :]
    lower_half = values[..., :half_dim]
    upper_half = values[..., half_dim:]
    return jnp.concatenate(
        [
            lower_half * cosine - upper_half * sine_part,
            upper_half * cosine + lower_half * sine_part,
        ],
        axis=-1,
    )


def carry_states(key_blocks, value_blocks, weighting, log_rates, block_size, backward):
    block_terms = jnp.einsum(
        "sbmhd,sbmhe->bshde",
        key_blocks * weighting[None, None, :, :, None],
        value_blocks,
        precision=highest_precision,
    )
    factor = jnp.exp(log_rates * block_size)[None, :, None, None]

    def advance(running, addend):
        return (running * factor + addend, running)

    initial = jnp.zeros(block_terms.shape[1:], jnp.float32)
    return lax.scan(advance, initial, block_terms, reverse=backward)[1]


def retain_blocks(
    query_rows, key_rows, value_rows, gate_rows, forward_decay, backward_decay, seq_count, length
):
    head_count = forward_decay.shape[0]
    head_dim = query_rows.shape[1] // head_count
    block_size = BLOCK
    block_count = length // block_size

    def split_heads(rows_in):
        return rows_in.astype(jnp.float32).reshape(seq_count, length, head_count, head_dim)

    def blocked(tensor):
        return tensor.reshape(seq_count, block_count, block_size, head_count, head_dim)

    queries = blocked(apply_rotary_heads(split_heads(query_rows), length))
    key_heads = blocked(apply_rotary_heads(split_heads(key_rows), length) * head_dim ** (-0.5))
    valued = blocked(split_heads(value_rows))
    rate_ahead = jax.nn.log_sigmoid(forward_decay)
    rate_behind = jax.nn.log_sigmoid(backward_decay)
    position = jnp.arange(block_size, dtype=jnp.float32)
    offset = position[:, None] - position[None, :]
    inside = jnp.where(
        offset[None] >= 0,
        jnp.exp(rate_ahead[:, None, None] * jnp.maximum(offset, 0.0)[None]),
        jnp.exp(rate_behind[:, None, None] * jnp.maximum(-offset, 0.0)[None]),
    )
    attention_scores = (
        jnp.einsum("sbchd,sbmhd->sbhcm", queries, key_heads, precision=highest_precision)
        * inside[None, None]
    )
    result = jnp.einsum("sbhcm,sbmhd->sbchd", attention_scores, valued, precision=highest_precision)
    column = position[:, None]
    key_ahead = jnp.exp(rate_ahead[None, :] * (block_size - 1 - column))
    query_ahead = jnp.exp(rate_ahead[None, :] * (column + 1))
    key_behind = jnp.exp(rate_behind[None, :] * column)
    query_behind = jnp.exp(rate_behind[None, :] * (block_size - column))
    from_before = carry_states(key_heads, valued, key_ahead, rate_ahead, block_size, False)
    from_after = carry_states(key_heads, valued, key_behind, rate_behind, block_size, True)
    result = (
        result
        + jnp.einsum("sbchd,bshde->sbche", queries, from_before, precision=highest_precision)
        * query_ahead[None, None, :, :, None]
    )
    result = (
        result
        + jnp.einsum("sbchd,bshde->sbche", queries, from_after, precision=highest_precision)
        * query_behind[None, None, :, :, None]
    )
    result = result.reshape(seq_count, length, head_count, head_dim)
    center = jnp.mean(result, axis=-1, keepdims=True)
    spread = jnp.mean(jnp.square(result - center), axis=-1, keepdims=True)
    normalized = (result - center) * lax.rsqrt(spread + group_eps)
    gated = jax.nn.silu(split_heads(gate_rows)) * normalized
    return gated.reshape(seq_count * length, head_count * head_dim).astype(jnp.bfloat16)


def accumulate(pieces, source):
    return tuple(
        (
            jnp.dot(source, weight_piece, preferred_element_type=jnp.float32)
            for weight_piece in pieces
        )
    )


def on_device(
    tokens,
    input_gain,
    query_weight,
    key_weight,
    value_weight,
    output_gate_matrix,
    forward_decay,
    backward_decay,
    merge_weight,
    middle_gain,
    gate_weight,
    up_weight,
    down_weight,
):
    seq_count, length, part_width = tokens.shape
    row_count = seq_count * length
    gathered = gathered_copies(tokens, "tp", 2)
    normed = rms_scale(gathered.reshape(row_count, gathered.shape[2]), input_gain)
    query_sum, key_sum, value_sum, gating_sum = accumulate(
        sent_together((query_weight, key_weight, value_weight, output_gate_matrix), "fs", 0, 1),
        normed,
    )
    mixed = retain_blocks(
        query_sum.astype(jnp.bfloat16),
        key_sum.astype(jnp.bfloat16),
        value_sum.astype(jnp.bfloat16),
        gating_sum.astype(jnp.bfloat16),
        forward_decay,
        backward_decay,
        seq_count,
        length,
    )
    merge_term = jnp.dot(
        mixed,
        lax.all_gather(merge_weight, "fs", axis=1, tiled=True),
        preferred_element_type=jnp.float32,
    )
    merged = summed_on_arrival(merge_term.astype(jnp.bfloat16), "tp", 1)
    middle = (tokens.reshape(row_count, part_width).astype(jnp.float32) + merged).astype(
        jnp.bfloat16
    )
    gathered_mid = gathered_copies(middle, "tp", 1)
    normed_mid = rms_scale(gathered_mid, middle_gain)
    gate_full, up_full = sent_together((gate_weight, up_weight), "fs", 0, 1)
    gate_act = jnp.dot(normed_mid, gate_full, preferred_element_type=jnp.float32)
    up_act = jnp.dot(normed_mid, up_full, preferred_element_type=jnp.float32)
    hidden = (jax.nn.silu(gate_act) * up_act).astype(jnp.bfloat16)
    down_term = jnp.dot(
        hidden,
        lax.all_gather(down_weight, "fs", axis=1, tiled=True),
        preferred_element_type=jnp.float32,
    )
    summed = summed_on_arrival(down_term.astype(jnp.bfloat16), "tp", 1)
    layer_out = (middle.astype(jnp.float32) + summed).astype(jnp.bfloat16)
    return layer_out.reshape(seq_count, length, part_width)


def solution(mesh):
    placed = (
        P(("grp", "fs"), None, "tp"),
        P(),
        P("fs", "tp"),
        P("fs", "tp"),
        P("fs", "tp"),
        P("fs", "tp"),
        P("tp"),
        P("tp"),
        P("tp", "fs"),
        P(),
        P("fs", "tp"),
        P("fs", "tp"),
        P("tp", "fs"),
    )
    return jax.shard_map(
        on_device,
        mesh=mesh,
        in_specs=placed,
        out_specs=P(("grp", "fs"), None, "tp"),
        check_vma=False,
    )
```

profile of v0, /device:TPU:40, one launch (start us, length us, event | category | flops | bytes accessed | tf_op | source)
XLA Modules:
  0.0 477.7 jit_solution(4488102892256830335)
XLA Ops:
  6.6 1.4 pad_maximum_fusion.2
  8.0 0.1 all-gather.4.cloned.1.call-update
  8.0 0.1 all-gather.6.cloned.1.call-start
  8.1 1.6 pad_maximum_fusion.1
  9.7 0.1 all-gather.6.cloned.1.call-update
  9.8 1.1 copy.41
  10.9 1.3 broadcast_in_dim.28
  12.1 4.7 all-to-all-start
  16.9 0.1 all-gather.8.cloned.1.call-start
  16.9 0.7 all-gather.8.cloned.1.call-update
  17.8 0.1 multiply_exponential_fusion
  17.9 0.1 multiply_exponential_fusion.1
  18.0 0.3 fusion.47
  18.3 0.1 exponential_select_fusion
  18.4 102.9 %all_gather.13 = bf16[128,2048]{0,1:T(8,128)(2,1)} all-gather(bf16[128,64]{0,1:T(8,128)(2,1)S(1)} %copy-done.2), channel_id=1, replica_groups=mesh['grp'=2,'fs'=32,'tp'=8] {'fs'}, dimensions={1}, use_global_device_ids=true | all-gather | bytes 540672 | tf_op jit(solution)/shard_map/all_gather | solution.py:190
  121.3 0.4 multiply_reduce_fusion.1
  121.7 0.2 bitcast_convert_fusion
  121.9 0.5 copy-done.3
  122.4 0.4 fusion.3
  122.8 47.4 %all-gather.4.cloned.1.call-done = bf16[2048,512]{1,0:T(8,128)(2,1)} async-done(((bf16[64,512]{1,0:T(8,128)(2,1)}), bf16[2048,512]{1,0:T(8,128)(2,1)}) %all-gather.4.cloned.1.call-update) | async-done | bytes 2097168 | tf_op jit(solution)/shard_map/all_gather | solution.py:32
  170.2 1.5 convolution_convert_fusion.3
  171.7 1.5 convolution_convert_fusion.2
  173.3 0.1 multiply_subtract_fusion.1
  173.4 1.7 convolution_convert_fusion.4
  175.1 0.1 reshape.440
  175.2 0.1 copy.47
  175.4 0.3 convolution_bitcast_fusion.4
  175.7 0.3 while.30
  175.7 0.1 bitcast_add_fusion.6
  175.8 0.1 bitcast_add_fusion.6
  175.9 0.1 bitcast_add_fusion.6
  176.0 0.1 reshape.425
  176.1 0.3 convolution_bitcast_fusion.3
  176.4 0.3 while.31
  176.4 0.1 bitcast_add_fusion.7
  176.5 0.1 bitcast_add_fusion.7
  176.6 0.1 bitcast_add_fusion.7
  176.7 0.8 convolution_multiply_fusion
  177.5 0.5 fusion.16
  178.0 0.5 fusion.17
  178.5 0.5 fusion.56
  179.0 0.2 copy.65
  179.3 0.9 reshape.439
  180.3 0.1 copy.59
  180.4 0.1 copy.58
  180.5 3.2 convolution_convert_fusion.1
  183.7 0.1 copy.82
  183.8 0.0 copy-start
  183.8 25.9 %all_to_all.20 = bf16[8,384,256]{2,1,0:T(8,128)(2,1)S(1)} all-to-all(bf16[8,384,256]{2,1,0:T(8,128)(2,1)S(1)} %bitcast.140), channel_id=1, replica_groups=mesh['grp'=2,'fs'=32,'tp'=8] {'tp'}, dimensions={0} | all-to-all | bytes 3145728 | tf_op jit(solution)/shard_map/all_to_all | solution.py:47
  209.7 0.2 convert_reduce_fusion.1
  210.0 0.2 copy.61
  210.2 0.1 broadcast_in_dim.33
  210.3 0.0 copy-start.4
  210.3 24.1 %all_to_all.21 = bf16[8,384,256]{1,2,0:T(8,128)(2,1)S(1)} all-to-all(bf16[8,384,256]{1,2,0:T(8,128)(2,1)S(1)} %broadcast_in_dim.33), channel_id=1, replica_groups=mesh['grp'=2,'fs'=32,'tp'=8] {'tp'}, dimensions={0} | all-to-all | bytes 3145728 | tf_op jit(solution)/shard_map/all_to_all | solution.py:23
  234.4 0.4 multiply_reduce_fusion
  234.9 0.4 fusion.1
  235.3 72.0 %all-gather.6.cloned.1.call-done = bf16[2048,1280]{1,0:T(8,128)(2,1)} async-done(((bf16[64,1280]{1,0:T(8,128)(2,1)}), bf16[2048,1280]{1,0:T(8,128)(2,1)}) %all-gather.6.cloned.1.call-update) | async-done | bytes 5242896 | tf_op jit(solution)/shard_map/all_gather | solution.py:32
  307.3 3.2 fusion.6
  310.5 127.6 %all-gather.8.cloned.1.call-done = bf16[640,2048]{0,1:T(8,128)(2,1)} async-done(((bf16[640,64]{0,1:T(8,128)(2,1)}), bf16[640,2048]{0,1:T(8,128)(2,1)}) %all-gather.8.cloned.1.call-update) | async-done | bytes 2621456 | tf_op jit(solution)/shard_map/all_gather | solution.py:205
  438.0 6.2 %convolution_convert_fusion = bf16[384,2048]{1,0:T(8,128)(2,1)S(1)} fusion(bf16[640,2048]{0,1:T(8,128)(2,1)} %all-gather.8.cloned.1.call-done, bf16[384,2048]{0,1:T(8,128)(2,1)} %copy-done.1, bf16[2048,1280]{1,0:T(8,128)(2,1)} %all-gather.6.cloned.1.call-done, f32[384,640]{1,0:T(8,128)S(1)} %fusion.6), kind=kOutput, calls=%fused_computation.14 | convolution fusion | flops 2015526912 | bytes 9371648 | tf_op jit(solution)/shard_map/dot_general | solution.py:203
  444.2 0.1 copy.81
  444.3 25.8 %all_to_all.22 = bf16[8,384,256]{2,1,0:T(8,128)(2,1)S(1)} all-to-all(bf16[8,384,256]{2,1,0:T(8,128)(2,1)S(1)} %bitcast.141), channel_id=1, replica_groups=mesh['grp'=2,'fs'=32,'tp'=8] {'tp'}, dimensions={0} | all-to-all | bytes 3145728 | tf_op jit(solution)/shard_map/all_to_all | solution.py:47
  470.2 0.2 convert_reduce_fusion
  470.4 0.8 fusion.26
  (44 shorter events, 0.5 us)
Async XLA Ops:
  6.5 163.6 %all-gather.4.cloned.1.call-start = ((), (), s32[]{:S(2)}) async-start(), calls=%async_computation.4 | async-start | bytes 2162688 | tf_op jit(solution)/shard_map/all_gather | solution.py:32
  8.0 299.3 %all-gather.6.cloned.1.call-start = ((), (), s32[]{:S(2)}) async-start(), calls=%async_computation.5 | async-start | bytes 5406720 | tf_op jit(solution)/shard_map/all_gather | solution.py:32
  12.1 5.7 %copy-start.5 = (f32[2]{0:T(128)S(1)}, f32[2]{0:T(128)}, u32[]{:S(2)}) copy-start(f32[2]{0:T(128)} %param.24) | copy-start | bytes 28
  12.1 5.7 %copy-start.6 = (f32[2]{0:T(128)S(1)}, f32[2]{0:T(128)}, u32[]{:S(2)}) copy-start(f32[2]{0:T(128)} %param.23) | copy-start | bytes 28
  12.1 6.2 %copy-start.2 = (bf16[128,64]{0,1:T(8,128)(2,1)S(1)}, bf16[128,64]{0,1:T(8,128)(2,1)}, u32[]{:S(2)}) copy-start(bf16[128,64]{0,1:T(8,128)(2,1)} %param.25) | copy-start | bytes 49156
  12.1 109.1 %all-to-all-start = ((bf16[8,1,384,256]{2,3,1,0:T(8,128)(2,1)}), bf16[8,1,384,256]{2,3,1,0:T(8,128)(2,1)S(1)}, u32[]{:S(2)}, u32[]{:S(2)}) async-start(bf16[8,1,384,256]{2,3,1,0:T(8,128)(2,1)} %broadcast_in_dim.28), calls=%async_computation | async-start | bytes 3145728 | tf_op jit(solution)/shard_map/all_to_all | solution.py:23
  16.9 421.2 %all-gather.8.cloned.1.call-start = ((), (), s32[]{:S(2)}) async-start(), calls=%async_computation.6 | async-start | bytes 2703360 | tf_op jit(solution)/shard_map/all_gather | solution.py:205
  121.7 0.7 copy-start.3
  183.8 26.1 %copy-start = (bf16[1,384,256]{2,1,0:T(8,128)(2,1)S(1)}, bf16[1,384,256]{2,1,0:T(8,128)(2,1)}, u32[]{:S(2)}) copy-start(bf16[1,384,256]{2,1,0:T(8,128)(2,1)} %param.17) | copy-start | bytes 589828
  210.3 24.5 %copy-start.4 = (f32[2048]{0:T(1024)S(1)}, f32[2048]{0:T(1024)}, u32[]{:S(2)}) copy-start(f32[2048]{0:T(1024)} %param.26) | copy-start | bytes 24580
  235.3 75.2 %copy-start.1 = (bf16[384,2048]{0,1:T(8,128)(2,1)}, bf16[384,2048]{0,1:T(8,128)(2,1)S(1)}, u32[]{:S(2)}) copy-start(bf16[384,2048]{0,1:T(8,128)(2,1)S(1)} %fusion.1) | copy-start | bytes 4718596
Sparse Core Ops, SparseCore 0:
  9.4 160.6 all-gather.3
  172.2 134.9 all-gather.5
  309.4 128.6 all-gather.7
where the time goes:
time: 479 us; the launch traced here: 478 us
  waiting for transfers between devices  248 us (52%)
  blocking collectives  179 us (37%)
  matrix products  20.1 us (4%)
  between operations  13.6 us (3%)
  other arithmetic  7.42 us (2%)
  local copies, waits for them, and re-layouts  5.27 us (1%)
  starting transfers between devices  4.84 us (1%)
    all_gather x1, waiting for transfers between devices, on_device(): lax.all_gather(down_weight, 'fs', axis=1, tiled=True)  128 us
    all_gather x2, waiting for transfers between devices, sent_together(): lax.all_gather(both, axis, axis=dim, tiled=True)  119 us
    all_gather x1, blocking collectives, on_device(): lax.all_gather(merge_weight, 'fs', axis=1, tiled=True)  103 us
    all_to_all x2, blocking collectives, summed_on_arrival(): tiles = lax.all_to_all(split_up(array, dim, peers), axis, 0, 0, tiled=True)  51.7 us
    all_to_all x1, blocking collectives, copy_for_each(): return lax.all_to_all(copies, axis, split_axis=0, concat_axis=0, tiled=True)  24.1 us
  transfers between devices with their start and end apart: 4, of which 3 were waited for; matrix products, arithmetic and copies ran while one was open for 5% of the time, Pallas kernels for 0%

commit v1 on v0

v1 whole, which is shorter than its diff:
```python
import functools

import jax
import jax.numpy as jnp
import numpy as np
from jax import lax
from jax.experimental import pallas as pl
from jax.experimental.pallas import tpu as pltpu
from jax.sharding import PartitionSpec as P

MESH = pl.DeviceIdType.MESH
HEAD = 64
NORM_EPS = 1e-06
GROUP_EPS = 1e-05
ROPE_BASE = 10000.0
F32 = jnp.float32
BF16 = jnp.bfloat16

NT_DIMS = (((1,), (1,)), ((), ()))


def rotation_tables(length):
    half = HEAD // 2
    inverse = ROPE_BASE ** (-np.arange(half, dtype=np.float32) / np.float32(half))
    angles = np.arange(length, dtype=np.float32)[:, None] * inverse.astype(np.float32)[None, :]
    cosine, sine = np.cos(angles), np.sin(angles)
    return (
        np.concatenate([cosine, cosine] * 2, axis=1).astype(np.float32),
        np.concatenate([-sine, sine] * 2, axis=1).astype(np.float32),
    )


def remote(src, dst, send_sem, recv_sem, device):
    return pltpu.make_async_remote_copy(
        src_ref=src, dst_ref=dst, send_sem=send_sem, recv_sem=recv_sem, device_id=device, device_id_type=MESH
    )


def layer_kernel(
    nf,
    nt,
    tok,
    gain1,
    wq,
    wk,
    wv,
    wo,
    fdec,
    bdec,
    wm,
    gain2,
    wgate,
    wup,
    wdown,
    cos,
    sin,
    out,
    a_buf,
    m_buf,
    g_buf,
    d_buf,
    m_stage,
    d_stage,
    tok_all,
    nrm,
    decay,
    qkvg,
    mixed,
    part,
    part_in,
    mid_all,
    hid,
    fin_out,
    fin_in,
    local_sem,
    ring_send,
    ring_recv,
    tok_send,
    tok_recv,
    part_send,
    part_recv,
    mid_send,
    mid_recv,
    fin_send,
    fin_recv,
):
    z = lax.axis_index("fs")
    t = lax.axis_index("tp")
    right, left = lax.rem(z + 1, nf), lax.rem(z + nf - 1, nf)
    far = nf // 2
    rows = tok.shape[0]
    width = tok.shape[1]
    per = wq.shape[0]
    cols = wq.shape[1]
    ff = wgate.shape[1]
    per_tp = width // per

    base = pl.multiple_of(z * per, per)
    mine = pl.ds(base, per)
    copies = [pltpu.make_async_copy(tok, tok_all.at[t], local_sem.at[0])]
    for n, w in enumerate((wq, wk, wv, wo)):
        copies.append(pltpu.make_async_copy(w, a_buf.at[mine, pl.ds(n * cols, cols)], local_sem.at[1 + n]))
    copies.append(pltpu.make_async_copy(wm, m_stage, local_sem.at[5]))
    copies.append(pltpu.make_async_copy(wgate, g_buf.at[mine, pl.ds(0, ff)], local_sem.at[6]))
    copies.append(pltpu.make_async_copy(wup, g_buf.at[mine, pl.ds(ff, ff)], local_sem.at[7]))
    copies.append(pltpu.make_async_copy(wdown, d_stage, local_sem.at[8]))
    for c in copies:
        c.start()

    barrier = pltpu.get_barrier_semaphore()
    for side in (left, right):
        pl.semaphore_signal(barrier, inc=1, device_id={"fs": side}, device_id_type=MESH)
    for k in range(1, nt):
        pl.semaphore_signal(barrier, inc=1, device_id={"tp": lax.rem(t + k, nt)}, device_id_type=MESH)
    pl.semaphore_wait(barrier, nt + 1)

    def hop(cls, s, wait_r, wait_l, send_r, send_l):
        buf, off, size, i = cls
        from_left = buf.at[pl.ds(pl.multiple_of(lax.rem(z - s + nf, nf) * per + off, 16), size)]
        from_right = buf.at[pl.ds(pl.multiple_of(lax.rem(z + s, nf) * per + off, 16), size)]
        if wait_r:
            remote(from_left, from_left, ring_send.at[i], ring_recv.at[i, 0, s], {"fs": left}).wait_recv()
        if send_r:
            remote(from_left, from_left, ring_send.at[i], ring_recv.at[i, 0, s + 1], {"fs": right}).start()
        if wait_l:
            remote(from_right, from_right, ring_send.at[i], ring_recv.at[i, 1, s], {"fs": right}).wait_recv()
        if send_l:
            remote(from_right, from_right, ring_send.at[i], ring_recv.at[i, 1, s + 1], {"fs": left}).start()

    def rounds(classes, lo, hi):
        if lo == 0 and hi > 0:
            for c in classes:
                hop(c, 0, False, False, True, True)
            lo = 1
        stop = min(hi, far - 1)
        if stop > lo:

            def body(s, carry):
                for c in classes:
                    hop(c, s, True, True, True, True)
                return carry

            lax.fori_loop(lo, stop, body, 0)
        if lo <= far - 1 < hi:
            for c in classes:
                hop(c, far - 1, True, True, True, False)
        if lo <= far < hi:
            for c in classes:
                hop(c, far, True, False, False, False)

    first = [(a_buf, 0, 32, 0), (a_buf, 32, 32, 1), (m_buf, 0, 64, 2), (g_buf, 0, 16, 3)]
    second = [(g_buf, 16, 16, 4), (g_buf, 32, 16, 5), (g_buf, 48, 16, 6)]
    third = [(d_buf, 0, 32, 7), (d_buf, 32, 32, 8)]

    def spread(buf, send_sem, recv_sem):
        def body(k, carry):
            j = lax.rem(t + k, nt)
            remote(buf.at[t], buf.at[t], send_sem.at[0], recv_sem.at[t], {"tp": j}).start()
            return carry

        lax.fori_loop(1, nt, body, 0)

    def arrived(buf, send_sem, recv_sem):
        def body(k, carry):
            j = lax.rem(t + k, nt)
            remote(buf.at[j], buf.at[j], send_sem.at[0], recv_sem.at[j], {"tp": j}).wait_recv()
            return carry

        lax.fori_loop(1, nt, body, 0)

    def normalize(src, gain):
        total = jnp.zeros((rows, 1), F32)
        for j in range(nt):
            v = src[j].astype(F32)
            total = total + jnp.sum(v * v, axis=-1, keepdims=True)
        scale = lax.rsqrt(total * (1.0 / (nt * width)) + NORM_EPS)
        for j in range(nt):
            span = pl.ds(j * width, width)
            nrm[:, span] = (src[j].astype(F32) * scale * gain[:, span]).astype(BF16)

    copies[0].wait()
    spread(tok_all, tok_send, tok_recv)
    for c in copies[1:5]:
        c.wait()
    rounds(first[:2], 0, 1)
    copies[5].wait()
    m_buf[mine, :] = m_stage[...].astype(F32).T.astype(BF16)
    copies[6].wait()
    copies[7].wait()
    rounds(first[3:], 0, 1)
    rounds(first[2:3], 0, 1)

    n_id = lax.broadcasted_iota(jnp.int32, (128, rows), 0)
    m_id = lax.broadcasted_iota(jnp.int32, (128, rows), 1)
    lane = lax.broadcasted_iota(jnp.int32, (rows, 2 * HEAD), 1)
    low_head = lane < HEAD
    fwd = jax.nn.log_sigmoid(fdec[...])
    bwd = jax.nn.log_sigmoid(bdec[...])
    for h in range(2):
        for c in range(rows // 128):
            gap = (n_id + (c * 128) - m_id).astype(F32)
            exponent = jnp.where(gap >= 0, fwd[:, h : h + 1] * gap, bwd[:, h : h + 1] * (-gap))
            decay[h, pl.ds(c * 128, 128), :] = jnp.exp(exponent)
        rounds(first, 1 + h, 2 + h)
    copies[8].wait()
    d_buf[mine, :] = d_stage[...].astype(F32).T.astype(BF16)
    rounds(first, 3, 7)
    arrived(tok_all, tok_send, tok_recv)
    normalize(tok_all, gain1)
    rounds(first, 7, far)
    rounds(second, 0, 1)
    rounds(first, far, far + 1)

    for n in range(4):
        span = pl.ds(n * cols, cols)
        qkvg[:, span] = jnp.dot(nrm[...], a_buf[:, span], preferred_element_type=F32).astype(BF16)
    rounds(second, 1, 2)

    def rotated(n):
        v = qkvg[:, pl.ds(n * cols, cols)].astype(F32)
        lo_half = lax.rem(lane, HEAD) < HEAD // 2
        swapped = jnp.where(lo_half, pltpu.roll(v, 2 * HEAD - HEAD // 2, 1), pltpu.roll(v, HEAD // 2, 1))
        return v * cos[...] + swapped * sin[...]

    rq = rotated(0)
    rk = (rotated(1) * HEAD**-0.5).astype(BF16)
    value = qkvg[:, pl.ds(2 * cols, cols)]
    rounds(second, 2, 3)
    kept = []
    for h in range(2):
        q_h = jnp.where(low_head if h == 0 else jnp.logical_not(low_head), rq, 0.0).astype(BF16)
        parts = []
        for c in range(rows // 128):
            scores = lax.dot_general(q_h[c * 128 : (c + 1) * 128], rk, NT_DIMS, preferred_element_type=F32)
            weighted = (scores * decay[h, pl.ds(c * 128, 128), :]).astype(BF16)
            parts.append(jnp.dot(weighted, value, preferred_element_type=F32))
        kept.append(jnp.concatenate(parts, axis=0))
        rounds(second, 3 + h, 4 + h)
    retained = jnp.where(low_head, kept[0], kept[1])

    def head_mean(v):
        lo = jnp.sum(jnp.where(low_head, v, 0.0), axis=-1, keepdims=True)
        hi = jnp.sum(jnp.where(low_head, 0.0, v), axis=-1, keepdims=True)
        return jnp.where(low_head, lo, hi) * (1.0 / HEAD)

    centered = retained - head_mean(retained)
    normalized = centered * lax.rsqrt(head_mean(centered * centered) + GROUP_EPS)
    gate = qkvg[:, pl.ds(3 * cols, cols)].astype(F32)
    mixed[...] = (gate / (1.0 + jnp.exp(-gate)) * normalized).astype(BF16)

    def project(k, carry):
        j = lax.rem(t + k, nt)
        w = m_buf[pl.ds(pl.multiple_of(j * width, width), width), :]
        part[j] = lax.dot_general(mixed[...], w, NT_DIMS, preferred_element_type=F32).astype(BF16)

        @pl.when(k < nt)
        def _():
            remote(part.at[j], part_in.at[t], part_send.at[0], part_recv.at[t], {"tp": j}).start()

        return carry

    lax.fori_loop(1, nt + 1, project, 0)
    rounds(second, 5, 11)

    def part_wait(k, carry):
        j = lax.rem(t + k, nt)
        remote(part.at[j], part_in.at[j], part_send.at[0], part_recv.at[j], {"tp": j}).wait_recv()
        return carry

    lax.fori_loop(1, nt, part_wait, 0)
    total = tok_all[t].astype(F32) + part[t].astype(F32)
    for k in range(1, nt):
        total = total + part_in[lax.rem(t + k, nt)].astype(F32)
    mid_all[t] = total.astype(BF16)
    rounds(second, 11, 12)
    spread(mid_all, mid_send, mid_recv)
    rounds(second, 12, far)
    rounds(third, 0, 1)
    rounds(second, far, far + 1)
    rounds(third, 1, 3)
    arrived(mid_all, mid_send, mid_recv)
    normalize(mid_all, gain2)
    at = 3
    for c in range(ff // 128):
        g = jnp.dot(nrm[...], g_buf[:, pl.ds(c * 128, 128)], preferred_element_type=F32)
        u = jnp.dot(nrm[...], g_buf[:, pl.ds(ff + c * 128, 128)], preferred_element_type=F32)
        hid[:, pl.ds(c * 128, 128)] = (g / (1.0 + jnp.exp(-g)) * u).astype(BF16)
        rounds(third, at, at + 1)
        at += 1

    def block(b):
        w = d_buf[pl.ds(pl.multiple_of(b * per, per), per), :]
        fin_out[b] = lax.dot_general(w, hid[...], NT_DIMS, preferred_element_type=F32).astype(BF16)
        j = lax.div(b, per_tp)
        q = b - j * per_tp

        @pl.when(j == t)
        def _():
            fin_in[t, q] = fin_out[b]

        @pl.when(j != t)
        def _():
            remote(fin_out.at[b], fin_in.at[t, q], fin_send.at[0], fin_recv.at[t, q], {"tp": j}).start()

    def pair(d):
        block(lax.rem(z - d + nf, nf))
        block(lax.rem(z + d, nf))

    block(z)
    done = 1
    span = far - at

    def catch_up(i, carry):
        for c in third:
            hop(c, at + i, True, True, True, True)
        pair(2 * i + 1)
        pair(2 * i + 2)
        return carry

    steps = far - 1 - at
    lax.fori_loop(0, steps, catch_up, 0)
    done = 2 * steps + 1
    rounds(third, far - 1, far)

    def rest(d, carry):
        pair(d)
        return carry

    lax.fori_loop(done, far, rest, 0)
    rounds(third, far, far + 1)
    block(lax.rem(z + far, nf))

    def fin_wait(k, carry):
        j = lax.rem(t + k, nt)
        for q in range(per_tp):
            remote(fin_out.at[0], fin_in.at[j, q], fin_send.at[0], fin_recv.at[j, q], {"tp": j}).wait_recv()
        return carry

    lax.fori_loop(1, nt, fin_wait, 0)
    for q in range(per_tp):
        total = fin_in[0, q].astype(F32)
        for j in range(1, nt):
            total = total + fin_in[j, q].astype(F32)
        fin_sum = total.T
        span_q = pl.ds(q * per, per)
        out[:, span_q] = (mid_all[t, :, span_q].astype(F32) + fin_sum).astype(BF16)

    for buf, off, size, i in first + second + third:
        whole = buf.at[pl.ds(0, (nf - 1) * size)]
        remote(whole, whole, ring_send.at[i], ring_recv.at[i, 0, 0], {"fs": right}).wait_send()
    for buf, sem in ((tok_all, tok_send), (part, part_send), (mid_all, mid_send)):
        whole = buf.at[pl.ds(0, nt - 1)]
        remote(whole, whole, sem.at[0], tok_recv.at[0], {"tp": lax.rem(t + 1, nt)}).wait_send()
    whole = fin_out.at[pl.ds(0, nf - per_tp)]
    remote(whole, whole, fin_send.at[0], fin_recv.at[0, 0], {"tp": lax.rem(t + 1, nt)}).wait_send()


def on_device(nf, nt, tokens, input_gain, wq, wk, wv, wo, fdec, bdec, wm, middle_gain, wgate, wup, wdown):
    seqs, rows, width = tokens.shape
    per, cols = wq.shape
    ff = wgate.shape[1]
    full = nf * per
    cos, sin = rotation_tables(rows)
    anywhere = pl.BlockSpec(memory_space=pl.ANY)
    vmem = pl.BlockSpec(memory_space=pltpu.VMEM)
    dma = pltpu.SemaphoreType.DMA
    out = pl.pallas_call(
        functools.partial(layer_kernel, nf, nt),
        out_shape=jax.ShapeDtypeStruct((rows, width), BF16),
        in_specs=[
            anywhere,
            vmem,
            anywhere,
            anywhere,
            anywhere,
            anywhere,
            vmem,
            vmem,
            anywhere,
            vmem,
            anywhere,
            anywhere,
            anywhere,
            vmem,
            vmem,
        ],
        out_specs=vmem,
        scratch_shapes=[
            pltpu.VMEM((full, 4 * cols), BF16),
            pltpu.VMEM((full, wm.shape[0]), BF16),
            pltpu.VMEM((full, 2 * ff), BF16),
            pltpu.VMEM((full, ff), BF16),
            pltpu.VMEM(wm.shape, BF16),
            pltpu.VMEM(wdown.shape, BF16),
            pltpu.VMEM((nt, rows, width), BF16),
            pltpu.VMEM((rows, full), BF16),
            pltpu.VMEM((2, rows, rows), F32),
            pltpu.VMEM((rows, 4 * cols), BF16),
            pltpu.VMEM((rows, cols), BF16),
            pltpu.VMEM((nt, rows, width), BF16),
            pltpu.VMEM((nt, rows, width), BF16),
            pltpu.VMEM((nt, rows, width), BF16),
            pltpu.VMEM((rows, ff), BF16),
            pltpu.VMEM((nf, per, rows), BF16),
            pltpu.VMEM((nt, width // per, per, rows), BF16),
            dma((9,)),
            dma((9,)),
            dma((9, 2, nf // 2 + 1)),
            dma((1,)),
            dma((nt,)),
            dma((1,)),
            dma((nt,)),
            dma((1,)),
            dma((nt,)),
            dma((1,)),
            dma((nt, width // per)),
        ],
        compiler_params=pltpu.CompilerParams(
            collective_id=0, has_side_effects=True, vmem_limit_bytes=60 * 1024 * 1024
        ),
    )(
        tokens.reshape(seqs * rows, width),
        input_gain.reshape(1, -1),
        wq,
        wk,
        wv,
        wo,
        fdec.reshape(1, -1),
        bdec.reshape(1, -1),
        wm,
        middle_gain.reshape(1, -1),
        wgate,
        wup,
        wdown,
        jnp.asarray(cos),
        jnp.asarray(sin),
    )
    return out.reshape(seqs, rows, width)


def solution(mesh):
    sizes = dict(mesh.shape)
    placed = (
        P(("grp", "fs"), None, "tp"),
        P(),
        P("fs", "tp"),
        P("fs", "tp"),
        P("fs", "tp"),
        P("fs", "tp"),
        P("tp"),
        P("tp"),
        P("tp", "fs"),
        P(),
        P("fs", "tp"),
        P("fs", "tp"),
        P("tp", "fs"),
    )
    return jax.shard_map(
        functools.partial(on_device, sizes["fs"], sizes["tp"]),
        mesh=mesh,
        in_specs=placed,
        out_specs=P(("grp", "fs"), None, "tp"),
        check_vma=False,
    )
```

time: 479 us -> 223 us (0.47)
  waiting for transfers between devices: 248 us -> 0 us
  Pallas kernels: 0 us -> 216 us
  blocking collectives: 179 us -> 0 us
  matrix products: 20.1 us -> 0 us
  between operations: 13.6 us -> 0.01 us
  other arithmetic: 7.42 us -> 0 us
  starting transfers between devices: 4.84 us -> 0 us
    all_gather x3 -> x0, waiting for transfers between devices: 247 us -> none  [the longest x1 128 us: on_device(): lax.all_gather(down_weight, 'fs', axis=1, tiled=True)]
    pallas_call x0 -> x1, Pallas kernels: none -> 216 us  [on_device(): pl.pallas_call(functools.partial(layer_kernel, nf, nt), out_shape=jax.Sha...]
    all_gather x1 -> x0, blocking collectives: 103 us -> none  [on_device(): lax.all_gather(merge_weight, 'fs', axis=1, tiled=True)]
    all_to_all x3 -> x0, blocking collectives: 75.8 us -> none  [the longest x2 51.7 us: summed_on_arrival(): tiles = lax.all_to_all(split_up(array, dim, peers), axis, 0, 0, tiled=True)]
    dot_general x12 -> x0, matrix products: 20.1 us -> none  [the longest x1 6.16 us: on_device(): jnp.dot(hidden, lax.all_gather(down_weight, 'fs', axis=1, tiled=True), pr...]
  transfers between devices with their start and end apart: 4 -> 0, of which waited for: 3 -> 0; matrix products, arithmetic and copies ran while one was open for 5% -> 0% of each run, Pallas kernels for 0% -> 0%
where the time goes in v1:
time: 223 us; the launch traced here: 221 us
  Pallas kernels  216 us (97%)
  local copies, waits for them, and re-layouts  4.72 us (2%)
    pallas_call x1, Pallas kernels, on_device(): pl.pallas_call(functools.partial(layer_kernel, nf, nt), out_shape=jax.Sha...  216 us
    unnamed x3, local copies, waits for them, and re-layouts  4.72 us

profile of v1, /device:TPU:40, one launch (start us, length us, event | category | flops | bytes accessed | tf_op | source)
XLA Modules:
  0.0 221.2 jit_solution(2325129090297939913)
XLA Ops:
  0.0 1.4 copy.16.wm
  1.4 1.7 copy.17.wdown
  3.1 216.5 %shard_map.145 = bf16[384,256]{1,0:T(8,128)(2,1)} custom-call(bf16[384,256]{1,0:T(8,128)(2,1)} %bitcast.7, f32[1,2048]{1,0:T(1,128)} %bitcast.8, bf16[64,128]{1,0:T(8,128)(2,1)} %wq.1, bf16[64,128]{1,0:T(8,128)(2,1)} %wk.1, bf16[64,128]{1,0:T(8,128)(2,1)} %wv.1, bf16[64,128]{1,0:T(8,128)(2,1)} %wo.1, f32[1,2]{1,0:T(1,128)} %bitcast.10, f32[1,2]{1,0:T(1,128)} %bitcast.11, ...), custom_call_target="tpu_custom_call" | custom-call | tf_op jit(solution)/shard_map/pallas_call | solution.py:367
  219.6 1.6 copy.19

commit v2 on v1

v2 whole, which is shorter than its diff:
```python
import functools

import jax
import jax.numpy as jnp
import numpy as np
from jax import lax
from jax.experimental import pallas as pl
from jax.experimental.pallas import tpu as pltpu
from jax.sharding import PartitionSpec as P

MESH = pl.DeviceIdType.MESH
HEAD = 64
NORM_EPS = 1e-06
GROUP_EPS = 1e-05
ROPE_BASE = 10000.0
F32 = jnp.float32
BF16 = jnp.bfloat16

D_START = 12

NT_DIMS = (((1,), (1,)), ((), ()))


def rotation_tables(length):
    half = HEAD // 2
    inverse = ROPE_BASE ** (-np.arange(half, dtype=np.float32) / np.float32(half))
    angles = np.arange(length, dtype=np.float32)[:, None] * inverse.astype(np.float32)[None, :]
    cosine, sine = np.cos(angles), np.sin(angles)
    return (
        np.concatenate([cosine, cosine] * 2, axis=1).astype(np.float32),
        np.concatenate([-sine, sine] * 2, axis=1).astype(np.float32),
    )


def remote(src, dst, send_sem, recv_sem, device):
    return pltpu.make_async_remote_copy(
        src_ref=src, dst_ref=dst, send_sem=send_sem, recv_sem=recv_sem, device_id=device, device_id_type=MESH
    )


def layer_kernel(
    nf,
    nt,
    tok,
    gain1,
    wq,
    wk,
    wv,
    wo,
    fdec,
    bdec,
    wm,
    gain2,
    wgate,
    wup,
    wdown,
    cos,
    sin,
    out,
    a_buf,
    g_buf,
    d_buf,
    tok_all,
    mid_all,
    nrm,
    decay,
    qacc,
    qkvg,
    mixed,
    acts,
    hid,
    own,
    ship1,
    got1,
    sums1,
    over1,
    last1,
    ship2,
    got2,
    sums2,
    over2,
    last2,
    local_sem,
    ring_send,
    ring_recv,
    pair_send,
    pair_recv,
    tok_send,
    tok_recv,
    mid_send,
    mid_recv,
    rs1_send,
    rs1_recv,
    rs2_send,
    rs2_recv,
):
    g = lax.axis_index("grp")
    z = lax.axis_index("fs")
    t = lax.axis_index("tp")
    nx = nt // 2
    x, c = lax.div(t, 2), lax.rem(t, 2)
    parity = lax.rem(g, 2)
    twin = {"grp": g + 1 - 2 * parity}
    right, left = {"fs": lax.rem(z + 1, nf)}, {"fs": lax.rem(z + nf - 1, nf)}

    def tp_of(dx, core):
        return lax.rem(x + dx + nx, nx) * 2 + core

    xr, xl, other = {"tp": tp_of(1, c)}, {"tp": tp_of(-1, c)}, {"tp": tp_of(0, 1 - c)}
    far = nf // 2
    rows, width = tok.shape
    half = rows // 2
    per, cols = wq.shape
    ff = wgate.shape[1]
    mcol = 4 * cols
    tiles = width // per

    mine = pl.ds(pl.multiple_of(z * per, per), per)
    copies = [pltpu.make_async_copy(tok, tok_all.at[t], local_sem.at[0])]
    for n, w in enumerate((wq, wk, wv, wo, wm)):
        copies.append(pltpu.make_async_copy(w, a_buf.at[mine, pl.ds(n * cols, cols)], local_sem.at[1 + n]))
    copies.append(pltpu.make_async_copy(wgate, g_buf.at[mine, pl.ds(0, ff)], local_sem.at[6]))
    copies.append(pltpu.make_async_copy(wup, g_buf.at[mine, pl.ds(ff, ff)], local_sem.at[7]))
    copies.append(pltpu.make_async_copy(wdown, d_buf.at[mine, :], local_sem.at[8]))
    for copy in copies:
        copy.start()

    barrier = pltpu.get_barrier_semaphore()
    for peer in (left, right, xl, xr, other, twin):
        pl.semaphore_signal(barrier, inc=1, device_id=peer, device_id_type=MESH)
    pl.semaphore_wait(barrier, 6)

    def shared(buf, row0, nrow, col0, ncol, by_row, i, k):
        step_r, step_c = (nrow, 0) if by_row else (0, ncol)
        flip = 1 - parity
        return (buf, row0 + step_r * parity, nrow, col0 + step_c * parity, ncol, i, k, row0 + step_r * flip, col0 + step_c * flip)

    g_common, g_half = 4 * 128, 3 * 128
    d_common, d_half = 128, 2 * 128
    cls_a = shared(a_buf, 0, per // 2, 0, mcol + wm.shape[1], True, 0, 0)
    cls_g0 = (g_buf, 0, per, 0, g_common, 1, None, 0, 0)
    cls_g1 = shared(g_buf, 0, per, g_common, g_half, False, 2, 1)
    cls_d0 = (d_buf, 0, per, 0, d_common, 3, None, 0, 0)
    cls_d1 = shared(d_buf, 0, per, d_common, d_half, False, 4, 2)

    def piece(cls, b, twins=False):
        buf, row0, nrow, col0, ncol, _, _, row1, col1 = cls
        r, k = (row1, col1) if twins else (row0, col0)
        r = pl.multiple_of(b * per + r, 16)
        k = k if isinstance(k, int) else pl.multiple_of(k, 128)
        return buf.at[pl.ds(r, nrow), pl.ds(k, ncol)]

    def hop(cls, s, wait_r, wait_l, send_r, send_l):
        i, k = cls[5], cls[6]
        for d, (b, source, target, wait, send) in enumerate(
            (
                (lax.rem(z - s + nf, nf), left, right, wait_r, send_r),
                (lax.rem(z + s, nf), right, left, wait_l, send_l),
            )
        ):
            ref = piece(cls, b)
            if wait:
                remote(ref, ref, ring_send.at[i], ring_recv.at[i, d, s], source).wait_recv()
            if send:
                remote(ref, ref, ring_send.at[i], ring_recv.at[i, d, s + 1], target).start()
            if wait and k is not None:
                remote(ref, ref, pair_send.at[k], pair_recv.at[k, d, s], twin).start()

    def from_twin(cls, lo, hi):
        k = cls[6]

        def one(s, d):
            b = lax.rem(z - s + nf, nf) if d == 0 else lax.rem(z + s, nf)
            ref = piece(cls, b, True)
            remote(ref, ref, pair_send.at[k], pair_recv.at[k, d, s], twin).wait_recv()

        def body(s, carry):
            one(s, 0)
            one(s, 1)
            return carry

        lax.fori_loop(lo, min(hi, far), body, 0)
        if hi > far:
            one(far, 0)

    classes = [(cls_a, 0), (cls_g0, 0), (cls_g1, 0), (cls_d0, D_START), (cls_d1, D_START)]
    clock = [0]

    def step_kind(s):
        if s < 0 or s > far:
            return None
        if s == 0:
            return (False, False, True, True)
        if s == far - 1:
            return (True, True, True, False)
        if s == far:
            return (True, False, False, False)
        return (True, True, True, True)

    def ticks(n):
        end = min(clock[0] + n, D_START + far + 1)
        while clock[0] < end:
            r = clock[0]
            kinds = [step_kind(r - off) for _, off in classes]
            run = r + 1
            if all(kind is None or kind == (True,) * 4 for kind in kinds):
                while run < end and [step_kind(run - off) for _, off in classes] == kinds:
                    run += 1

                def body(q, carry):
                    for (cls, off), kind in zip(classes, kinds):
                        if kind is not None:
                            hop(cls, q - off, *kind)
                    return carry

                lax.fori_loop(r, run, body, 0)
            else:
                for (cls, off), kind in zip(classes, kinds):
                    if kind is not None:
                        hop(cls, r - off, *kind)
            clock[0] = run

    sent = []

    def put(src, dst, send, recv, i, device):
        copy = remote(src, dst, send.at[i], recv.at[i], device)
        copy.start()
        sent.append(copy)

    def got(dst, send, recv, i, device):
        remote(dst, dst, send.at[i], recv.at[i], device).wait_recv()

    halves = (pl.ds(0, half), pl.ds(half, half))

    def gather_start(buf, send, recv):
        for h in (0, 1):
            part = buf.at[t, halves[h]]
            put(part, part, send, recv, h, xr)
            part = buf.at[t, halves[1 - h]]
            put(part, part, send, recv, 3 - h, xl)
        put(buf.at[t], buf.at[t], send, recv, 6, other)

    def gather_rest(buf, send, recv, pause):
        block_l, block_r, block_o = tp_of(-1, c), tp_of(1, c), tp_of(2, c)
        for i, block, h, source, onward, j in (
            (0, block_l, 0, xl, xr, 4),
            (3, block_r, 1, xr, xl, 5),
            (1, block_l, 1, xl, None, None),
            (2, block_r, 0, xr, None, None),
            (4, block_o, 0, xl, None, None),
            (5, block_o, 1, xr, None, None),
        ):
            if i in (1, 4):
                pause()
            part = buf.at[block, halves[h]]
            got(part, send, recv, i, source)
            if onward is not None:
                put(part, part, send, recv, j, onward)
            put(part, part, send, recv, 7 + i, other)
        pause()
        got(buf.at[tp_of(0, 1 - c)], send, recv, 6, other)
        for i, dx, h in ((0, -1, 0), (1, -1, 1), (2, 1, 0), (3, 1, 1), (4, 2, 0), (5, 2, 1)):
            got(buf.at[tp_of(dx, 1 - c), halves[h]], send, recv, 7 + i, other)

    def reduce_scatter(partial, ship, have, sums, over, last, send, recv, pause):
        for r, dx in enumerate((2, 1, -1, 0)):
            ship[r] = partial(tp_of(dx, 1 - c)).astype(BF16)
            put(ship.at[r], have.at[r], send, recv, r, other)
            own[r] = partial(tp_of(dx, c))
        pause()
        got(have.at[0], send, recv, 0, other)
        sums[0] = (own[0] + have[0].astype(F32)).astype(BF16)
        put(sums.at[0, halves[0]], over.at[0], send, recv, 4, xr)
        put(sums.at[0, halves[1]], over.at[1], send, recv, 5, xl)
        got(have.at[1], send, recv, 1, other)
        sums[1, halves[1]] = (own[1, halves[1]] + have[1, halves[1]].astype(F32)).astype(BF16)
        put(sums.at[1, halves[1]], last.at[0, halves[1]], send, recv, 6, xr)
        got(have.at[2], send, recv, 2, other)
        sums[2, halves[0]] = (own[2, halves[0]] + have[2, halves[0]].astype(F32)).astype(BF16)
        put(sums.at[2, halves[0]], last.at[1, halves[0]], send, recv, 7, xl)
        got(have.at[3], send, recv, 3, other)
        own[3] = own[3] + have[3].astype(F32)
        pause()
        got(over.at[0], send, recv, 4, xl)
        sums[1, halves[0]] = (own[1, halves[0]] + have[1, halves[0]].astype(F32) + over[0].astype(F32)).astype(BF16)
        put(sums.at[1, halves[0]], last.at[0, halves[0]], send, recv, 8, xr)
        got(over.at[1], send, recv, 5, xr)
        sums[2, halves[1]] = (own[2, halves[1]] + have[2, halves[1]].astype(F32) + over[1].astype(F32)).astype(BF16)
        put(sums.at[2, halves[1]], last.at[1, halves[1]], send, recv, 9, xl)
        pause()
        got(last.at[0, halves[1]], send, recv, 6, xl)
        got(last.at[1, halves[0]], send, recv, 7, xr)
        got(last.at[0, halves[0]], send, recv, 8, xl)
        got(last.at[1, halves[1]], send, recv, 9, xr)
        return own[3] + last[0].astype(F32) + last[1].astype(F32)

    def normalize(source, gain):
        total = jnp.zeros((rows, 1), F32)
        for j in range(nt):
            v = source[j].astype(F32)
            total = total + jnp.sum(v * v, axis=-1, keepdims=True)
        scale = lax.rsqrt(total * (1.0 / (nt * width)) + NORM_EPS)
        for j in range(nt):
            span = pl.ds(j * width, width)
            nrm[:, span] = (source[j].astype(F32) * scale * gain[:, span]).astype(BF16)

    for copy in copies[1:6]:
        copy.wait()
    hop(cls_a, 0, False, False, True, True)
    copies[0].wait()
    gather_start(tok_all, tok_send, tok_recv)
    for copy in copies[6:]:
        copy.wait()
    hop(cls_g0, 0, False, False, True, True)
    hop(cls_g1, 0, False, False, True, True)
    clock[0] = 1

    n_id = lax.broadcasted_iota(jnp.int32, (128, rows), 0)
    m_id = lax.broadcasted_iota(jnp.int32, (128, rows), 1)
    lane = lax.broadcasted_iota(jnp.int32, (rows, 2 * HEAD), 1)
    low_head = lane < HEAD
    fwd = jax.nn.log_sigmoid(fdec[...])
    bwd = jax.nn.log_sigmoid(bdec[...])
    for h in range(2):
        for chunk in range(rows // 128):
            gap = (n_id + (chunk * 128) - m_id).astype(F32)
            exponent = jnp.where(gap >= 0, fwd[:, h : h + 1] * gap, bwd[:, h : h + 1] * (-gap))
            decay[h, pl.ds(chunk * 128, 128), :] = jnp.exp(exponent)
    ticks(1)
    gather_rest(tok_all, tok_send, tok_recv, lambda: ticks(1))
    normalize(tok_all, gain1)

    first = lax.div(z, tiles)

    def add_group(k, start=False):
        j = lax.rem(first + k + nt, nt)
        rows_j = pl.ds(pl.multiple_of(j * width, width), width)
        term = jnp.dot(
            nrm[:, pl.ds(pl.multiple_of(j * width, width), width)], a_buf[rows_j, pl.ds(0, mcol)], preferred_element_type=F32
        )
        qacc[...] = term if start else qacc[...] + term

    for k in range(far // tiles):
        ticks(tiles * k + tiles + 1 - clock[0])
        if k == 0:
            from_twin(cls_a, 1, tiles)
            add_group(0, True)
        else:
            from_twin(cls_a, tiles * k, tiles * k + tiles)
            add_group(k)
            add_group(-k)
    ticks(far + 1 - clock[0])
    from_twin(cls_a, far, far + 1)
    add_group(far // tiles)
    qkvg[...] = qacc[...].astype(BF16)
    ticks(1)

    def rotated(n):
        v = qkvg[:, pl.ds(n * cols, cols)].astype(F32)
        lo_half = lax.rem(lane, HEAD) < HEAD // 2
        swapped = jnp.where(lo_half, pltpu.roll(v, 2 * HEAD - HEAD // 2, 1), pltpu.roll(v, HEAD // 2, 1))
        return v * cos[...] + swapped * sin[...]

    rq = rotated(0)
    rk = (rotated(1) * HEAD**-0.5).astype(BF16)
    value = qkvg[:, pl.ds(2 * cols, cols)]
    kept = []
    for h in range(2):
        q_h = jnp.where(low_head if h == 0 else jnp.logical_not(low_head), rq, 0.0).astype(BF16)
        parts = []
        for chunk in range(rows // 128):
            scores = lax.dot_general(q_h[chunk * 128 : (chunk + 1) * 128], rk, NT_DIMS, preferred_element_type=F32)
            weighted = (scores * decay[h, pl.ds(chunk * 128, 128), :]).astype(BF16)
            parts.append(jnp.dot(weighted, value, preferred_element_type=F32))
        kept.append(jnp.concatenate(parts, axis=0))
    ticks(1)
    retained = jnp.where(low_head, kept[0], kept[1])

    def head_mean(v):
        lo = jnp.sum(jnp.where(low_head, v, 0.0), axis=-1, keepdims=True)
        hi = jnp.sum(jnp.where(low_head, 0.0, v), axis=-1, keepdims=True)
        return jnp.where(low_head, lo, hi) * (1.0 / HEAD)

    centered = retained - head_mean(retained)
    normalized = centered * lax.rsqrt(head_mean(centered * centered) + GROUP_EPS)
    gate = qkvg[:, pl.ds(3 * cols, cols)].astype(F32)
    mixed[...] = (gate / (1.0 + jnp.exp(-gate)) * normalized).astype(BF16)

    def merge_part(j):
        w = a_buf[pl.ds(pl.multiple_of(j * width, width), width), pl.ds(mcol, wm.shape[1])]
        return lax.dot_general(mixed[...], w, NT_DIMS, preferred_element_type=F32)

    merged = reduce_scatter(merge_part, ship1, got1, sums1, over1, last1, rs1_send, rs1_recv, lambda: ticks(1))
    mid_all[t] = (tok_all[t].astype(F32) + merged).astype(BF16)
    gather_start(mid_all, mid_send, mid_recv)
    gather_rest(mid_all, mid_send, mid_recv, lambda: ticks(1))
    normalize(mid_all, gain2)
    from_twin(cls_g1, 1, far + 1)
    acts[:, pl.ds(0, ff)] = jnp.dot(nrm[...], g_buf[:, pl.ds(0, ff)], preferred_element_type=F32)
    ticks(1)
    acts[:, pl.ds(ff, ff)] = jnp.dot(nrm[...], g_buf[:, pl.ds(ff, ff)], preferred_element_type=F32)
    ticks(1)
    gated = acts[:, pl.ds(0, ff)]
    hid[...] = (gated / (1.0 + jnp.exp(-gated)) * acts[:, pl.ds(ff, ff)]).astype(BF16)
    ticks(D_START + far + 1)
    from_twin(cls_d1, 1, far + 1)

    def down_part(j):
        w = d_buf[pl.ds(pl.multiple_of(j * width, width), width), :]
        return lax.dot_general(hid[...], w, NT_DIMS, preferred_element_type=F32)

    summed = reduce_scatter(down_part, ship2, got2, sums2, over2, last2, rs2_send, rs2_recv, lambda: None)
    out[...] = (mid_all[t].astype(F32) + summed).astype(BF16)

    for cls, _ in classes:
        buf, row0, nrow, col0, ncol, i, k, _, _ = cls
        cut = pl.ds(col0 if isinstance(col0, int) else pl.multiple_of(col0, 128), ncol)
        whole = buf.at[pl.ds(0, (nf - 1) * nrow), cut]
        remote(whole, whole, ring_send.at[i], ring_recv.at[i, 0, 0], right).wait_send()
        if k is not None:
            remote(whole, whole, pair_send.at[k], pair_recv.at[k, 0, 0], twin).wait_send()
    for copy in sent:
        copy.wait_send()


def on_device(nf, nt, tokens, input_gain, wq, wk, wv, wo, fdec, bdec, wm, middle_gain, wgate, wup, wdown):
    seqs, rows, width = tokens.shape
    per, cols = wq.shape
    ff = wgate.shape[1]
    full = nf * per
    nx = nt // 2
    cos, sin = rotation_tables(rows)
    anywhere = pl.BlockSpec(memory_space=pl.ANY)
    vmem = pl.BlockSpec(memory_space=pltpu.VMEM)
    dma = pltpu.SemaphoreType.DMA
    block = (rows, width)
    exchange = [
        pltpu.VMEM((nx, *block), BF16),
        pltpu.VMEM((nx, *block), BF16),
        pltpu.VMEM((3, *block), BF16),
        pltpu.VMEM((2, rows // 2, width), BF16),
        pltpu.VMEM((2, *block), BF16),
    ]
    out = pl.pallas_call(
        functools.partial(layer_kernel, nf, nt),
        out_shape=jax.ShapeDtypeStruct(block, BF16),
        in_specs=[anywhere, vmem]
        + [anywhere] * 4
        + [vmem, vmem, anywhere, vmem]
        + [anywhere] * 3
        + [vmem, vmem],
        out_specs=vmem,
        scratch_shapes=[
            pltpu.VMEM((full, 4 * cols + wm.shape[0]), BF16),
            pltpu.VMEM((full, 2 * ff), BF16),
            pltpu.VMEM((full, ff), BF16),
            pltpu.VMEM((nt, *block), BF16),
            pltpu.VMEM((nt, *block), BF16),
            pltpu.VMEM((rows, full), BF16),
            pltpu.VMEM((2, rows, rows), F32),
            pltpu.VMEM((rows, 4 * cols), F32),
            pltpu.VMEM((rows, 4 * cols), BF16),
            pltpu.VMEM((rows, cols), BF16),
            pltpu.VMEM((rows, 2 * ff), F32),
            pltpu.VMEM((rows, ff), BF16),
            pltpu.VMEM((nx, *block), F32),
            *exchange,
            *exchange,
            dma((9,)),
            dma((5,)),
            dma((5, 2, nf // 2 + 1)),
            dma((3,)),
            dma((3, 2, nf // 2 + 1)),
            dma((13,)),
            dma((13,)),
            dma((13,)),
            dma((13,)),
            dma((10,)),
            dma((10,)),
            dma((10,)),
            dma((10,)),
        ],
        compiler_params=pltpu.CompilerParams(
            collective_id=0, has_side_effects=True, vmem_limit_bytes=60 * 1024 * 1024
        ),
    )(
        tokens.reshape(seqs * rows, width),
        input_gain.reshape(1, -1),
        wq,
        wk,
        wv,
        wo,
        fdec.reshape(1, -1),
        bdec.reshape(1, -1),
        wm.T,
        middle_gain.reshape(1, -1),
        wgate,
        wup,
        wdown.T,
        jnp.asarray(cos),
        jnp.asarray(sin),
    )
    return out.reshape(seqs, rows, width)


def solution(mesh):
    sizes = dict(mesh.shape)
    placed = (
        P(("grp", "fs"), None, "tp"),
        P(),
        P("fs", "tp"),
        P("fs", "tp"),
        P("fs", "tp"),
        P("fs", "tp"),
        P("tp"),
        P("tp"),
        P("tp", "fs"),
        P(),
        P("fs", "tp"),
        P("fs", "tp"),
        P("tp", "fs"),
    )
    return jax.shard_map(
        functools.partial(on_device, sizes["fs"], sizes["tp"]),
        mesh=mesh,
        in_specs=placed,
        out_specs=P(("grp", "fs"), None, "tp"),
        check_vma=False,
    )
```

time: 223 us -> 178 us (0.80)
  Pallas kernels: 216 us -> 176 us
  local copies, waits for them, and re-layouts: 4.72 us -> 1.62 us
    pallas_call x1, Pallas kernels: 216 us -> 176 us  [on_device(): pl.pallas_call(functools.partial(layer_kernel, nf, nt), out_shape=jax.Sha...]
    unnamed x3 -> x1, local copies, waits for them, and re-layouts: 4.72 us -> 1.62 us
where the time goes in v2:
time: 178 us; the launch traced here: 177 us
  Pallas kernels  176 us (99%)
    pallas_call x1, Pallas kernels, on_device(): pl.pallas_call(functools.partial(layer_kernel, nf, nt), out_shape=jax.Sha...  176 us

profile of v2, /device:TPU:40, one launch (start us, length us, event | category | flops | bytes accessed | tf_op | source)
XLA Modules:
  0.0 177.3 jit_solution(514361184363161857)
XLA Ops:
  0.0 175.7 %shard_map.145 = bf16[384,256]{1,0:T(8,128)(2,1)} custom-call(bf16[384,256]{1,0:T(8,128)(2,1)} %bitcast.9, f32[1,2048]{1,0:T(1,128)} %bitcast.12, bf16[64,128]{1,0:T(8,128)(2,1)} %wq.1, bf16[64,128]{1,0:T(8,128)(2,1)} %wk.1, bf16[64,128]{1,0:T(8,128)(2,1)} %wv.1, bf16[64,128]{1,0:T(8,128)(2,1)} %wo.1, f32[1,2]{1,0:T(1,128)} %bitcast.14, f32[1,2]{1,0:T(1,128)} %bitcast.15, ...), custom_call_target="tpu_custom_call" | custom-call | tf_op jit(solution)/shard_map/pallas_call | solution.py:444
  175.7 1.6 copy.17

commit v3 on v2

--- a/solution.py
+++ b/solution.py
@@ -16,7 +16,9 @@
 F32 = jnp.float32
 BF16 = jnp.bfloat16
 
-D_START = 12
+D_START = 0
+SLOTS = 4
+STRIDE = 3
 
 NT_DIMS = (((1,), (1,)), ((), ()))
 
@@ -81,6 +83,10 @@
     over2,
     last2,
     local_sem,
+    far_send,
+    far_recv,
+    far_pair_send,
+    far_pair_recv,
     ring_send,
     ring_recv,
     pair_send,
@@ -102,6 +108,7 @@
     parity = lax.rem(g, 2)
     twin = {"grp": g + 1 - 2 * parity}
     right, left = {"fs": lax.rem(z + 1, nf)}, {"fs": lax.rem(z + nf - 1, nf)}
+    right_far, left_far = {"fs": lax.rem(z + STRIDE, nf)}, {"fs": lax.rem(z + nf - STRIDE, nf)}
 
     def tp_of(dx, core):
         return lax.rem(x + dx + nx, nx) * 2 + core
@@ -126,9 +133,9 @@
         copy.start()
 
     barrier = pltpu.get_barrier_semaphore()
-    for peer in (left, right, xl, xr, other, twin):
+    for peer in (left, right, left_far, right_far, xl, xr, other, twin):
         pl.semaphore_signal(barrier, inc=1, device_id=peer, device_id_type=MESH)
-    pl.semaphore_wait(barrier, 6)
+    pl.semaphore_wait(barrier, 8)
 
     def shared(buf, row0, nrow, col0, ncol, by_row, i, k):
         step_r, step_c = (nrow, 0) if by_row else (0, ncol)
@@ -137,11 +144,16 @@
 
     g_common, g_half = 4 * 128, 3 * 128
     d_common, d_half = 128, 2 * 128
-    cls_a = shared(a_buf, 0, per // 2, 0, mcol + wm.shape[1], True, 0, 0)
-    cls_g0 = (g_buf, 0, per, 0, g_common, 1, None, 0, 0)
-    cls_g1 = shared(g_buf, 0, per, g_common, g_half, False, 2, 1)
-    cls_d0 = (d_buf, 0, per, 0, d_common, 3, None, 0, 0)
-    cls_d1 = shared(d_buf, 0, per, d_common, d_half, False, 4, 2)
+    lower = per // 2
+    cls_a = shared(a_buf, 0, lower, 0, mcol + wm.shape[1], True, None, None)
+    cls_g = shared(g_buf, 0, per, g_common, g_half, False, None, 0)
+    cls_d = shared(d_buf, 0, per, d_common, d_half, False, 5, 1)
+    cls_g0 = (g_buf, 0, lower, 0, g_common, 0, None, 0, 0)
+    cls_g1 = (g_buf, lower, lower, 0, g_common, 1, None, 0, 0)
+    cls_g2 = shared(g_buf, 0, lower, g_common, g_half, False, 2, None)
+    cls_g3 = shared(g_buf, lower, lower, g_common, g_half, False, 3, None)
+    cls_d0 = (d_buf, 0, per, 0, d_common, 4, None, 0, 0)
+    paired = {3: cls_g, 5: cls_d}
 
     def piece(cls, b, twins=False):
         buf, row0, nrow, col0, ncol, _, _, row1, col1 = cls
@@ -151,7 +163,7 @@
         return buf.at[pl.ds(r, nrow), pl.ds(k, ncol)]
 
     def hop(cls, s, wait_r, wait_l, send_r, send_l):
-        i, k = cls[5], cls[6]
+        i = cls[5]
         for d, (b, source, target, wait, send) in enumerate(
             (
                 (lax.rem(z - s + nf, nf), left, right, wait_r, send_r),
@@ -160,10 +172,11 @@
         ):
             ref = piece(cls, b)
             if wait:
-                remote(ref, ref, ring_send.at[i], ring_recv.at[i, d, s], source).wait_recv()
+                remote(ref, ref, ring_send.at[i], ring_recv.at[i, d, lax.rem(s, SLOTS)], source).wait_recv()
             if send:
-                remote(ref, ref, ring_send.at[i], ring_recv.at[i, d, s + 1], target).start()
-            if wait and k is not None:
+                remote(ref, ref, ring_send.at[i], ring_recv.at[i, d, lax.rem(s + 1, SLOTS)], target).start()
+            if wait and i in paired:
+                ref, k = piece(paired[i], b), paired[i][6]
                 remote(ref, ref, pair_send.at[k], pair_recv.at[k, d, s], twin).start()
 
     def from_twin(cls, lo, hi):
@@ -183,7 +196,50 @@
         if hi > far:
             one(far, 0)
 
-    classes = [(cls_a, 0), (cls_g0, 0), (cls_g1, 0), (cls_d0, D_START), (cls_d1, D_START)]
+    stages = (far - 1) // STRIDE
+
+    def at_distance(d, twins=False):
+        return piece(cls_a, lax.rem(z - d + nf, nf), twins)
+
+    def pass_on(d, step, device):
+        ref = at_distance(d)
+        remote(ref, ref, far_send.at[0], far_recv.at[d + step + far - 1], device).start()
+
+    def receive(d):
+        ref = at_distance(d)
+        remote(ref, ref, far_send.at[0], far_recv.at[d + far - 1], right).wait_recv()
+
+    def to_twin(d):
+        ref = at_distance(d)
+        remote(ref, ref, far_pair_send.at[0], far_pair_recv.at[d + far - 1], twin).start()
+
+    def twin_blocks(lo, hi):
+        for dist in range(lo, hi):
+            for d in (dist, -dist) if dist < far else (dist,):
+                ref = at_distance(d, True)
+                remote(ref, ref, far_pair_send.at[0], far_pair_recv.at[d + far - 1], twin).wait_recv()
+
+    def stage(i):
+        for sign, ahead, behind, jump in ((1, right, left, right_far), (-1, left, right, left_far)):
+            d = sign * STRIDE * i
+            if i > 0:
+                receive(d)
+            if i < stages:
+                pass_on(d, sign * STRIDE, jump)
+            if abs(d) + 1 < far or sign > 0:
+                pass_on(d, sign, ahead)
+            if i > 0:
+                pass_on(d, -sign, behind)
+                to_twin(d)
+
+    def fills(i):
+        near = [1, -1] if i == 0 else [STRIDE * i - 1, 1 - STRIDE * i, STRIDE * i + 1, -STRIDE * i - 1]
+        for d in near:
+            if d > -far:
+                receive(d)
+                to_twin(d)
+
+    classes = [(cls_g0, 0), (cls_g1, 0), (cls_g2, 0), (cls_g3, 0), (cls_d0, D_START), (cls_d, D_START)]
     clock = [0]
 
     def step_kind(s):
@@ -220,15 +276,11 @@
                         hop(cls, r - off, *kind)
             clock[0] = run
 
-    sent = []
-
     def put(src, dst, send, recv, i, device):
-        copy = remote(src, dst, send.at[i], recv.at[i], device)
-        copy.start()
-        sent.append(copy)
+        remote(src, dst, send.at[0], recv.at[i], device).start()
 
     def got(dst, send, recv, i, device):
-        remote(dst, dst, send.at[i], recv.at[i], device).wait_recv()
+        remote(dst, dst, send.at[0], recv.at[i], device).wait_recv()
 
     halves = (pl.ds(0, half), pl.ds(half, half))
 
@@ -263,21 +315,26 @@
             got(buf.at[tp_of(dx, 1 - c), halves[h]], send, recv, 7 + i, other)
 
     def reduce_scatter(partial, ship, have, sums, over, last, send, recv, pause):
-        for r, dx in enumerate((2, 1, -1, 0)):
+        def product(r, dx):
             ship[r] = partial(tp_of(dx, 1 - c)).astype(BF16)
             put(ship.at[r], have.at[r], send, recv, r, other)
             own[r] = partial(tp_of(dx, c))
-        pause()
+
+        product(0, 2)
+        product(1, 1)
         got(have.at[0], send, recv, 0, other)
         sums[0] = (own[0] + have[0].astype(F32)).astype(BF16)
         put(sums.at[0, halves[0]], over.at[0], send, recv, 4, xr)
         put(sums.at[0, halves[1]], over.at[1], send, recv, 5, xl)
+        product(2, -1)
         got(have.at[1], send, recv, 1, other)
         sums[1, halves[1]] = (own[1, halves[1]] + have[1, halves[1]].astype(F32)).astype(BF16)
         put(sums.at[1, halves[1]], last.at[0, halves[1]], send, recv, 6, xr)
+        product(3, 0)
         got(have.at[2], send, recv, 2, other)
         sums[2, halves[0]] = (own[2, halves[0]] + have[2, halves[0]].astype(F32)).astype(BF16)
         put(sums.at[2, halves[0]], last.at[1, halves[0]], send, recv, 7, xl)
+        pause()
         got(have.at[3], send, recv, 3, other)
         own[3] = own[3] + have[3].astype(F32)
         pause()
@@ -304,32 +361,6 @@
             span = pl.ds(j * width, width)
             nrm[:, span] = (source[j].astype(F32) * scale * gain[:, span]).astype(BF16)
 
-    for copy in copies[1:6]:
-        copy.wait()
-    hop(cls_a, 0, False, False, True, True)
-    copies[0].wait()
-    gather_start(tok_all, tok_send, tok_recv)
-    for copy in copies[6:]:
-        copy.wait()
-    hop(cls_g0, 0, False, False, True, True)
-    hop(cls_g1, 0, False, False, True, True)
-    clock[0] = 1
-
-    n_id = lax.broadcasted_iota(jnp.int32, (128, rows), 0)
-    m_id = lax.broadcasted_iota(jnp.int32, (128, rows), 1)
-    lane = lax.broadcasted_iota(jnp.int32, (rows, 2 * HEAD), 1)
-    low_head = lane < HEAD
-    fwd = jax.nn.log_sigmoid(fdec[...])
-    bwd = jax.nn.log_sigmoid(bdec[...])
-    for h in range(2):
-        for chunk in range(rows // 128):
-            gap = (n_id + (chunk * 128) - m_id).astype(F32)
-            exponent = jnp.where(gap >= 0, fwd[:, h : h + 1] * gap, bwd[:, h : h + 1] * (-gap))
-            decay[h, pl.ds(chunk * 128, 128), :] = jnp.exp(exponent)
-    ticks(1)
-    gather_rest(tok_all, tok_send, tok_recv, lambda: ticks(1))
-    normalize(tok_all, gain1)
-
     first = lax.div(z, tiles)
 
     def add_group(k, start=False):
@@ -340,17 +371,61 @@
         )
         qacc[...] = term if start else qacc[...] + term
 
-    for k in range(far // tiles):
-        ticks(tiles * k + tiles + 1 - clock[0])
-        if k == 0:
-            from_twin(cls_a, 1, tiles)
-            add_group(0, True)
-        else:
-            from_twin(cls_a, tiles * k, tiles * k + tiles)
-            add_group(k)
-            add_group(-k)
-    ticks(far + 1 - clock[0])
-    from_twin(cls_a, far, far + 1)
+    n_id = lax.broadcasted_iota(jnp.int32, (128, rows), 0)
+    m_id = lax.broadcasted_iota(jnp.int32, (128, rows), 1)
+    lane = lax.broadcasted_iota(jnp.int32, (rows, 2 * HEAD), 1)
+    low_head = lane < HEAD
+
+    def decay_weights(h):
+        fwd = jax.nn.log_sigmoid(fdec[...])
+        bwd = jax.nn.log_sigmoid(bdec[...])
+        for chunk in range(rows // 128):
+            gap = (n_id + (chunk * 128) - m_id).astype(F32)
+            exponent = jnp.where(gap >= 0, fwd[:, h : h + 1] * gap, bwd[:, h : h + 1] * (-gap))
+            decay[h, pl.ds(chunk * 128, 128), :] = jnp.exp(exponent)
+
+    for copy in copies[1:6]:
+        copy.wait()
+    stage(0)
+    copies[0].wait()
+    gather_start(tok_all, tok_send, tok_recv)
+    for copy in copies[6:]:
+        copy.wait()
+    ticks(1)
+    decay_weights(0)
+    stage(1)
+    ticks(1)
+    fills(0)
+    decay_weights(1)
+    stage(2)
+    ticks(1)
+    fills(1)
+    gather_rest(tok_all, tok_send, tok_recv, lambda: None)
+    ticks(1)
+    stage(3)
+    ticks(1)
+    fills(2)
+    normalize(tok_all, gain1)
+    ticks(1)
+    stage(4)
+    ticks(1)
+    fills(3)
+    twin_blocks(1, 2 * tiles)
+    add_group(0, True)
+    ticks(1)
+    stage(5)
+    ticks(1)
+    fills(4)
+    add_group(1)
+    add_group(-1)
+    fills(5)
+    ticks(1)
+    twin_blocks(2 * tiles, 3 * tiles)
+    add_group(2)
+    add_group(-2)
+    twin_blocks(3 * tiles, far + 1)
+    add_group(3)
+    add_group(-3)
     add_group(far // tiles)
     qkvg[...] = qacc[...].astype(BF16)
     ticks(1)
@@ -395,7 +470,8 @@
     gather_start(mid_all, mid_send, mid_recv)
     gather_rest(mid_all, mid_send, mid_recv, lambda: ticks(1))
     normalize(mid_all, gain2)
-    from_twin(cls_g1, 1, far + 1)
+    ticks(far + 1 - clock[0])
+    from_twin(cls_g, 1, far + 1)
     acts[:, pl.ds(0, ff)] = jnp.dot(nrm[...], g_buf[:, pl.ds(0, ff)], preferred_element_type=F32)
     ticks(1)
     acts[:, pl.ds(ff, ff)] = jnp.dot(nrm[...], g_buf[:, pl.ds(ff, ff)], preferred_element_type=F32)
@@ -403,7 +479,7 @@
     gated = acts[:, pl.ds(0, ff)]
     hid[...] = (gated / (1.0 + jnp.exp(-gated)) * acts[:, pl.ds(ff, ff)]).astype(BF16)
     ticks(D_START + far + 1)
-    from_twin(cls_d1, 1, far + 1)
+    from_twin(cls_d, 1, far + 1)
 
     def down_part(j):
         w = d_buf[pl.ds(pl.multiple_of(j * width, width), width), :]
@@ -412,15 +488,22 @@
     summed = reduce_scatter(down_part, ship2, got2, sums2, over2, last2, rs2_send, rs2_recv, lambda: None)
     out[...] = (mid_all[t].astype(F32) + summed).astype(BF16)
 
+    whole = a_buf.at[pl.ds(0, (nf - 1) * (per // 2)), :]
+    remote(whole, whole, far_send.at[0], far_recv.at[0], right).wait_send()
+    remote(whole, whole, far_pair_send.at[0], far_pair_recv.at[0], twin).wait_send()
+    def drain(cls, sem, recv, device):
+        buf, row0, nrow, col0, ncol = cls[:5]
+        cut = pl.ds(col0 if isinstance(col0, int) else pl.multiple_of(col0, 128), ncol)
+        total = buf.at[pl.ds(0, (nf - 1) * nrow), cut]
+        remote(total, total, sem, recv, device).wait_send()
+
     for cls, _ in classes:
-        buf, row0, nrow, col0, ncol, i, k, _, _ = cls
-        cut = pl.ds(col0 if isinstance(col0, int) else pl.multiple_of(col0, 128), ncol)
-        whole = buf.at[pl.ds(0, (nf - 1) * nrow), cut]
-        remote(whole, whole, ring_send.at[i], ring_recv.at[i, 0, 0], right).wait_send()
-        if k is not None:
-            remote(whole, whole, pair_send.at[k], pair_recv.at[k, 0, 0], twin).wait_send()
-    for copy in sent:
-        copy.wait_send()
+        drain(cls, ring_send.at[cls[5]], ring_recv.at[cls[5], 0, 0], right)
+    for cls in paired.values():
+        drain(cls, pair_send.at[cls[6]], pair_recv.at[cls[6], 0, 0], twin)
+    whole = tok_all.at[pl.ds(0, nt - 1)]
+    for sem in (tok_send, mid_send, rs1_send, rs2_send):
+        remote(whole, whole, sem.at[0], tok_recv.at[0], other).wait_send()
 
 
 def on_device(nf, nt, tokens, input_gain, wq, wk, wv, wo, fdec, bdec, wm, middle_gain, wgate, wup, wdown):
@@ -467,17 +550,21 @@
             *exchange,
             *exchange,
             dma((9,)),
-            dma((5,)),
-            dma((5, 2, nf // 2 + 1)),
-            dma((3,)),
-            dma((3, 2, nf // 2 + 1)),
+            dma((1,)),
+            dma((nf,)),
+            dma((1,)),
+            dma((nf,)),
+            dma((6,)),
+            dma((6, 2, SLOTS)),
+            dma((2,)),
+            dma((2, 2, nf // 2 + 1)),
+            dma((1,)),
             dma((13,)),
+            dma((1,)),
             dma((13,)),
-            dma((13,)),
-            dma((13,)),
+            dma((1,)),
             dma((10,)),
-            dma((10,)),
-            dma((10,)),
+            dma((1,)),
             dma((10,)),
         ],
         compiler_params=pltpu.CompilerParams(

time: 178 us -> 164 us (0.921)
  Pallas kernels: 176 us -> 161 us
    pallas_call x1, Pallas kernels: 176 us -> 161 us  [on_device(): pl.pallas_call(functools.partial(layer_kernel, nf, nt), out_shape=jax.Sha...]
where the time goes in v3:
time: 164 us; the launch traced here: 163 us
  Pallas kernels  161 us (98%)
    pallas_call x1, Pallas kernels, on_device(): pl.pallas_call(functools.partial(layer_kernel, nf, nt), out_shape=jax.Sha...  161 us

profile of v3, /device:TPU:40, one launch (start us, length us, event | category | flops | bytes accessed | tf_op | source)
XLA Modules:
  0.0 162.7 jit_solution(5705565084034541570)
XLA Ops:
  0.0 161.1 %shard_map.145 = bf16[384,256]{1,0:T(8,128)(2,1)} custom-call(bf16[384,256]{1,0:T(8,128)(2,1)} %bitcast.9, f32[1,2048]{1,0:T(1,128)} %bitcast.12, bf16[64,128]{1,0:T(8,128)(2,1)} %wq.1, bf16[64,128]{1,0:T(8,128)(2,1)} %wk.1, bf16[64,128]{1,0:T(8,128)(2,1)} %wv.1, bf16[64,128]{1,0:T(8,128)(2,1)} %wo.1, f32[1,2]{1,0:T(1,128)} %bitcast.14, f32[1,2]{1,0:T(1,128)} %bitcast.15, ...), custom_call_target="tpu_custom_call" | custom-call | tf_op jit(solution)/shard_map/pallas_call | solution.py:527
  161.1 1.6 copy.17

commit v4 on v3

--- a/solution.py
+++ b/solution.py
@@ -64,6 +64,7 @@
     d_buf,
     tok_all,
     mid_all,
+    nrm_in,
     nrm,
     decay,
     qacc,
@@ -330,11 +331,11 @@
         got(have.at[1], send, recv, 1, other)
         sums[1, halves[1]] = (own[1, halves[1]] + have[1, halves[1]].astype(F32)).astype(BF16)
         put(sums.at[1, halves[1]], last.at[0, halves[1]], send, recv, 6, xr)
+        pause()
         product(3, 0)
         got(have.at[2], send, recv, 2, other)
         sums[2, halves[0]] = (own[2, halves[0]] + have[2, halves[0]].astype(F32)).astype(BF16)
         put(sums.at[2, halves[0]], last.at[1, halves[0]], send, recv, 7, xl)
-        pause()
         got(have.at[3], send, recv, 3, other)
         own[3] = own[3] + have[3].astype(F32)
         pause()
@@ -351,7 +352,7 @@
         got(last.at[1, halves[1]], send, recv, 9, xr)
         return own[3] + last[0].astype(F32) + last[1].astype(F32)
 
-    def normalize(source, gain):
+    def normalize(source, gain, store):
         total = jnp.zeros((rows, 1), F32)
         for j in range(nt):
             v = source[j].astype(F32)
@@ -359,16 +360,14 @@
         scale = lax.rsqrt(total * (1.0 / (nt * width)) + NORM_EPS)
         for j in range(nt):
             span = pl.ds(j * width, width)
-            nrm[:, span] = (source[j].astype(F32) * scale * gain[:, span]).astype(BF16)
+            store(j, (source[j].astype(F32) * scale * gain[:, span]).astype(BF16))
 
     first = lax.div(z, tiles)
 
     def add_group(k, start=False):
         j = lax.rem(first + k + nt, nt)
         rows_j = pl.ds(pl.multiple_of(j * width, width), width)
-        term = jnp.dot(
-            nrm[:, pl.ds(pl.multiple_of(j * width, width), width)], a_buf[rows_j, pl.ds(0, mcol)], preferred_element_type=F32
-        )
+        term = jnp.dot(nrm_in[j], a_buf[rows_j, pl.ds(0, mcol)], preferred_element_type=F32)
         qacc[...] = term if start else qacc[...] + term
 
     n_id = lax.broadcasted_iota(jnp.int32, (128, rows), 0)
@@ -401,11 +400,10 @@
     ticks(1)
     fills(1)
     gather_rest(tok_all, tok_send, tok_recv, lambda: None)
-    ticks(1)
     stage(3)
     ticks(1)
     fills(2)
-    normalize(tok_all, gain1)
+    normalize(tok_all, gain1, lambda j, v: nrm_in.__setitem__(j, v))
     ticks(1)
     stage(4)
     ticks(1)
@@ -414,7 +412,6 @@
     add_group(0, True)
     ticks(1)
     stage(5)
-    ticks(1)
     fills(4)
     add_group(1)
     add_group(-1)
@@ -448,7 +445,6 @@
             weighted = (scores * decay[h, pl.ds(chunk * 128, 128), :]).astype(BF16)
             parts.append(jnp.dot(weighted, value, preferred_element_type=F32))
         kept.append(jnp.concatenate(parts, axis=0))
-    ticks(1)
     retained = jnp.where(low_head, kept[0], kept[1])
 
     def head_mean(v):
@@ -469,7 +465,7 @@
     mid_all[t] = (tok_all[t].astype(F32) + merged).astype(BF16)
     gather_start(mid_all, mid_send, mid_recv)
     gather_rest(mid_all, mid_send, mid_recv, lambda: ticks(1))
-    normalize(mid_all, gain2)
+    normalize(mid_all, gain2, lambda j, v: nrm.__setitem__((slice(None), pl.ds(j * width, width)), v))
     ticks(far + 1 - clock[0])
     from_twin(cls_g, 1, far + 1)
     acts[:, pl.ds(0, ff)] = jnp.dot(nrm[...], g_buf[:, pl.ds(0, ff)], preferred_element_type=F32)
@@ -537,6 +533,7 @@
             pltpu.VMEM((full, 4 * cols + wm.shape[0]), BF16),
             pltpu.VMEM((full, 2 * ff), BF16),
             pltpu.VMEM((full, ff), BF16),
+            pltpu.VMEM((nt, *block), BF16),
             pltpu.VMEM((nt, *block), BF16),
             pltpu.VMEM((nt, *block), BF16),
             pltpu.VMEM((rows, full), BF16),

time: 164 us -> 162 us (0.988)
  no operation moved by 1% of the time
where the time goes in v4:
time: 162 us; the launch traced here: 161 us
  Pallas kernels  160 us (99%)
  local copies, waits for them, and re-layouts  1.62 us (1%)
    pallas_call x1, Pallas kernels, on_device(): pl.pallas_call(functools.partial(layer_kernel, nf, nt), out_shape=jax.Sha...  160 us

profile of v4, /device:TPU:40, one launch (start us, length us, event | category | flops | bytes accessed | tf_op | source)
XLA Modules:
  0.0 161.2 jit_solution(10529087581407882386)
XLA Ops:
  0.0 159.6 %shard_map.145 = bf16[384,256]{1,0:T(8,128)(2,1)} custom-call(bf16[384,256]{1,0:T(8,128)(2,1)} %bitcast.9, f32[1,2048]{1,0:T(1,128)} %bitcast.12, bf16[64,128]{1,0:T(8,128)(2,1)} %wq.1, bf16[64,128]{1,0:T(8,128)(2,1)} %wk.1, bf16[64,128]{1,0:T(8,128)(2,1)} %wv.1, bf16[64,128]{1,0:T(8,128)(2,1)} %wo.1, f32[1,2]{1,0:T(1,128)} %bitcast.14, f32[1,2]{1,0:T(1,128)} %bitcast.15, ...), custom_call_target="tpu_custom_call" | custom-call | tf_op jit(solution)/shard_map/pallas_call | solution.py:523
  159.6 1.6 %copy.17 = bf16[1,384,256]{2,1,0:T(8,128)(2,1)} copy(bf16[1,384,256]{2,1,0:T(8,128)(2,1)} %bitcast.8) | data formatting | bytes 393216

commit v5 on v4

--- a/solution.py
+++ b/solution.py
@@ -240,7 +240,7 @@
                 receive(d)
                 to_twin(d)
 
-    classes = [(cls_g0, 0), (cls_g1, 0), (cls_g2, 0), (cls_g3, 0), (cls_d0, D_START), (cls_d, D_START)]
+    classes = [(cls_d0, D_START), (cls_g2, 0), (cls_g3, 0), (cls_g0, 0), (cls_g1, 0), (cls_d, D_START)]
     clock = [0]
 
     def step_kind(s):

time: 162 us -> 161 us (level)
  Pallas kernels: 160 us -> 158 us
where the time goes in v5:
time: 161 us; the launch traced here: 160 us
  Pallas kernels  158 us (98%)
  local copies, waits for them, and re-layouts  1.62 us (1%)
    pallas_call x1, Pallas kernels, on_device(): pl.pallas_call(functools.partial(layer_kernel, nf, nt), out_shape=jax.Sha...  158 us

profile of v5, /device:TPU:40, one launch (start us, length us, event | category | flops | bytes accessed | tf_op | source)
XLA Modules:
  0.0 159.9 jit_solution(13081742377913791200)
XLA Ops:
  0.0 158.2 %shard_map.145 = bf16[384,256]{1,0:T(8,128)(2,1)} custom-call(bf16[384,256]{1,0:T(8,128)(2,1)} %bitcast.9, f32[1,2048]{1,0:T(1,128)} %bitcast.12, bf16[64,128]{1,0:T(8,128)(2,1)} %wq.1, bf16[64,128]{1,0:T(8,128)(2,1)} %wk.1, bf16[64,128]{1,0:T(8,128)(2,1)} %wv.1, bf16[64,128]{1,0:T(8,128)(2,1)} %wo.1, f32[1,2]{1,0:T(1,128)} %bitcast.14, f32[1,2]{1,0:T(1,128)} %bitcast.15, ...), custom_call_target="tpu_custom_call" | custom-call | tf_op jit(solution)/shard_map/pallas_call | solution.py:523
  158.2 1.6 %copy.17 = bf16[1,384,256]{2,1,0:T(8,128)(2,1)} copy(bf16[1,384,256]{2,1,0:T(8,128)(2,1)} %bitcast.8) | data formatting | bytes 393216
